TPU v7x, 32 devices: a whole 2x2x4 slice. The times are simulated.
32 devices in a mesh: ep: 4 (over z), tp: 8 (over y, x, core).
Axes of the slice: x: 2, y: 2, z: 4, core: 2. Of those that a mesh axis runs over, the one named last changes fastest.
Arguments:
- hidden_in: bfloat16 [48, 2048], P('ep', 'tp'), may hold values from -12 to 12
- state: float32 [48, 32, 128, 128], P('ep', 'tp'), may hold values from -3 to 3
- lower_bound: float32 [32, 128], P('tp'), may hold values from 0.05 to 0.95
- w_forget: bfloat16 [2048, 4096], P(None, 'tp'), may hold values from -0.125 to 0.125
- w_input: bfloat16 [2048, 4096], P(None, 'tp'), may hold values from -0.125 to 0.125
- w_query: bfloat16 [2048, 4096], P(None, 'tp'), may hold values from -0.125 to 0.125
- w_outgate: bfloat16 [2048, 4096], P(None, 'tp'), may hold values from -0.125 to 0.125
- head_gain: float32 [128], replicated, may hold values from 0.1 to 1.9
- w_out: bfloat16 [4096, 2048], P('tp'), may hold values from -0.125 to 0.125
- ln1_gain: float32 [2048], replicated, may hold values from 0.1 to 8
- ln1_bias: float32 [2048], replicated, may hold values from -1.5 to 1.5
- routes: int32 [48, 4], P('ep'), may hold values from 0 to 7, all different within a row; in each aligned block of 12 rows (0 to 11, 12 to 23, ...) at most 9 rows name the same one
- route_weights: float32 [48, 4], P('ep'), may hold values from 0.2 to 1.5
- exp_gate: bfloat16 [8, 2048, 4096], P('ep', None, 'tp'), may hold values from -0.125 to 0.125
- exp_up: bfloat16 [8, 2048, 4096], P('ep', None, 'tp'), may hold values from -0.125 to 0.125
- exp_down: bfloat16 [8, 4096, 2048], P('ep', 'tp'), may hold values from -0.125 to 0.125
- sh_gate: bfloat16 [2048, 512], P(None, 'tp'), may hold values from -0.125 to 0.125
- sh_up: bfloat16 [2048, 512], P(None, 'tp'), may hold values from -0.125 to 0.125
- sh_down: bfloat16 [512, 2048], P('tp'), may hold values from -0.25 to 0.25
- ln2_gain: float32 [2048], replicated, may hold values from 0.1 to 1.9
- ln2_bias: float32 [2048], replicated, may hold values from -1.5 to 1.5
Outputs:
- mixed_out: bfloat16 [48, 2048], P('ep', 'tp')
- new_state: float32 [48, 32, 128, 128], P('ep', 'tp')
Inputs may be any that keep to these rules, and one draw needn't show every extreme that they name: `routes`: each row names 4 different experts; among the rows of one index of ep (12 rows) no expert is named more than 9 times, a bound that some block reaches.
All inputs are finite; a program needn't handle non-finite values.
Results may differ from a plain program's by a relative error of at most 0.023.
Values may be sent and summed in bfloat16 or wider, within the bound.
A program may use at most 64 MiB of HBM per device.

v0:
```python
import jax
import jax.numpy as jnp
from jax import lax
from jax.sharding import PartitionSpec as P

EPS = 1e-05
ALPHA = 2.0**0.25


def rounded(value):
    return lax.optimization_barrier(value.astype(jnp.bfloat16)).astype(jnp.float32)


def local(
    hidden_in,
    state,
    lower_bound,
    w_forget,
    w_input,
    w_query,
    w_outgate,
    head_gain,
    w_out,
    ln1_gain,
    ln1_bias,
    routes,
    route_weights,
    exp_gate,
    exp_up,
    exp_down,
    sh_gate,
    sh_up,
    sh_down,
    ln2_gain,
    ln2_bias,
):
    n_tp = lax.axis_size("tp")
    n_ep = lax.axis_size("ep")
    seq_count = hidden_in.shape[0]
    col_count = hidden_in.shape[1]
    model_width = col_count * n_tp
    col_start = lax.axis_index("tp") * col_count
    heads_dev = state.shape[1]
    head_size = state.shape[2]
    top_count = routes.shape[1]
    local_experts = exp_gate.shape[0]
    expert_count = local_experts * n_ep
    capacity = max(2, 3 * seq_count * top_count // (2 * expert_count))
    slot_count = expert_count * capacity
    rows_full = lax.all_gather(hidden_in, "tp", axis=1, tiled=True)

    def project(weight):
        product = jnp.dot(rows_full, weight, preferred_element_type=jnp.float32)
        return rounded(product).reshape(seq_count, heads_dev, head_size)

    forget_pre = project(w_forget)
    forget = lower_bound + (1.0 - lower_bound) * jax.nn.sigmoid(forget_pre)
    key_part = (1.0 - lower_bound) * jax.nn.sigmoid(-forget_pre)
    values = project(w_input)
    queries = jax.nn.silu(project(w_query))
    out_gate = jax.nn.silu(project(w_outgate))
    new_state = forget[..., None] * state + key_part[..., None] * values[:, :, None, :]
    readout = jnp.einsum("bhd,bhdv->bhv", queries, new_state, precision=lax.Precision.HIGHEST)
    normed = readout * lax.rsqrt(jnp.mean(readout * readout, -1, keepdims=True) + EPS) * head_gain
    mixed = (normed * out_gate).astype(jnp.bfloat16).reshape(seq_count, heads_dev * head_size)
    branch = jnp.dot(mixed, w_out, preferred_element_type=jnp.float32)
    summed = lax.psum(branch.astype(jnp.bfloat16), "tp").astype(jnp.float32)
    residual = ALPHA * rows_full.astype(jnp.float32) + summed
    average = jnp.mean(residual, -1, keepdims=True)
    centered = residual - average
    variance = jnp.mean(centered * centered, -1, keepdims=True)
    normed_rows = (centered * lax.rsqrt(variance + EPS) * ln1_gain + ln1_bias).astype(jnp.bfloat16)
    routes_flat = routes.reshape(-1)
    one_hot = (routes_flat[:, None] == jnp.arange(expert_count, dtype=jnp.int32)[None, :]).astype(
        jnp.int32
    )
    position = jnp.sum((jnp.cumsum(one_hot, 0) - one_hot) * one_hot, 1)
    slot_index = routes_flat * capacity + position
    placing = (slot_index[:, None] == jnp.arange(slot_count, dtype=jnp.int32)[None, :]).astype(
        jnp.float32
    )
    chooser = jnp.sum(placing.reshape(seq_count, top_count, slot_count), 1).astype(jnp.bfloat16)
    weighted = jnp.sum(
        (placing * route_weights.reshape(-1)[:, None]).reshape(seq_count, top_count, slot_count), 1
    )
    own_cols = lax.dynamic_slice_in_dim(normed_rows, col_start, col_count, 1)
    picked = lax.dot_general(
        chooser, normed_rows, (((0,), (0,)), ((), ())), preferred_element_type=jnp.float32
    )
    arrived = lax.all_to_all(
        picked.astype(jnp.bfloat16).reshape(n_ep, local_experts * capacity, normed_rows.shape[1]),
        "ep",
        split_axis=0,
        concat_axis=0,
        tiled=True,
    )
    blocks = arrived.reshape(n_ep, local_experts, capacity, model_width)
    gate_part = jnp.einsum("gecd,edf->gecf", blocks, exp_gate, preferred_element_type=jnp.float32)
    up_part = jnp.einsum("gecd,edf->gecf", blocks, exp_up, preferred_element_type=jnp.float32)
    hidden_part = (jax.nn.silu(gate_part) * up_part).astype(jnp.bfloat16)
    expert_part = jnp.einsum(
        "gecf,efd->gecd", hidden_part, exp_down, preferred_element_type=jnp.float32
    )
    expert_part = expert_part.reshape(n_ep, local_experts * capacity, model_width).astype(
        jnp.bfloat16
    )
    shared_hidden = (
        jax.nn.silu(jnp.dot(normed_rows, sh_gate, preferred_element_type=jnp.float32))
        * jnp.dot(normed_rows, sh_up, preferred_element_type=jnp.float32)
    ).astype(jnp.bfloat16)
    shared_part = jnp.dot(shared_hidden, sh_down, preferred_element_type=jnp.float32)
    returned = lax.all_to_all(expert_part, "ep", split_axis=0, concat_axis=0, tiled=True)
    routed_partial = jnp.dot(
        weighted,
        returned.reshape(slot_count, model_width).astype(jnp.float32),
        precision=lax.Precision.HIGHEST,
    )
    combined = lax.psum_scatter(
        (routed_partial + shared_part).astype(jnp.bfloat16), "tp", scatter_dimension=1, tiled=True
    ).astype(jnp.float32)
    final_in = ALPHA * own_cols.astype(jnp.float32) + combined
    moments_two = lax.psum((jnp.sum(final_in, -1), jnp.sum(final_in * final_in, -1)), "tp")
    average_two = moments_two[0][:, None] / model_width
    variance_two = moments_two[1][:, None] / model_width - average_two * average_two
    gain_two = lax.dynamic_slice_in_dim(ln2_gain, col_start, col_count)
    bias_two = lax.dynamic_slice_in_dim(ln2_bias, col_start, col_count)
    mixed_out = (
        (final_in - average_two) * lax.rsqrt(variance_two + EPS) * gain_two + bias_two
    ).astype(jnp.bfloat16)
    return (mixed_out, new_state)


def solution(mesh):
    placed = (
        P("ep", "tp"),
        P("ep", "tp", None, None),
        P("tp", None),
        P(None, "tp"),
        P(None, "tp"),
        P(None, "tp"),
        P(None, "tp"),
        P(),
        P("tp", None),
        P(),
        P(),
        P("ep", None),
        P("ep", None),
        P("ep", None, "tp"),
        P("ep", None, "tp"),
        P("ep", "tp", None),
        P(None, "tp"),
        P(None, "tp"),
        P("tp", None),
        P(),
        P(),
    )
    return jax.shard_map(
        local,
        mesh=mesh,
        in_specs=placed,
        out_specs=(P("ep", "tp"), P("ep", "tp", None, None)),
        check_vma=False,
    )
```

profile of v0, /device:TPU:0, one launch (start us, length us, event | category | flops | bytes accessed | tf_op | source)
XLA Modules:
  0.0 155.0 jit_solution(1456552702936218920)
XLA Ops:
  7.2 0.9 copy.41
  8.6 0.8 copy.43
  9.4 10.7 %all_gather.3 = bf16[12,2048]{1,0:T(8,128)(2,1)S(1)} all-gather(bf16[12,256]{1,0:T(8,128)(2,1)} %param.21), channel_id=1, replica_groups=mesh['ep'=4,'tp'=8] {'tp'}, dimensions={1}, use_global_device_ids=true | all-gather | bytes 55296 | tf_op jit(solution)/shard_map/all_gather | solution.py:50
  20.1 2.0 %convolution_convert_fusion.2 = bf16[12,512]{1,0:T(8,128)(2,1)S(1)} fusion(bf16[12,2048]{1,0:T(8,128)(2,1)S(1)} %all_gather.3, bf16[2048,512]{1,0:T(8,128)(2,1)} %param.27), kind=kOutput, calls=%fused_computation.17 | convolution fusion | flops 25171968 | bytes 2158592 | tf_op jit(solution)/shard_map/dot_general | solution.py:53
  22.1 2.0 %convolution_convert_fusion.5 = bf16[12,512]{1,0:T(8,128)(2,1)S(1)} fusion(bf16[12,2048]{1,0:T(8,128)(2,1)S(1)} %all_gather.3, bf16[2048,512]{1,0:T(8,128)(2,1)} %param.26), kind=kOutput, calls=%fused_computation.20 | convolution fusion | flops 25171968 | bytes 2158592 | tf_op jit(solution)/shard_map/dot_general | solution.py:53
  24.1 2.0 %convolution_convert_fusion.3 = bf16[12,512]{1,0:T(8,128)(2,1)S(1)} fusion(bf16[12,2048]{1,0:T(8,128)(2,1)S(1)} %all_gather.3, bf16[2048,512]{1,0:T(8,128)(2,1)} %param.25), kind=kOutput, calls=%fused_computation.18 | convolution fusion | flops 25171968 | bytes 2158592 | tf_op jit(solution)/shard_map/dot_general | solution.py:53
  26.1 2.0 %convolution_convert_fusion.4 = bf16[12,512]{1,0:T(8,128)(2,1)S(1)} fusion(bf16[12,2048]{1,0:T(8,128)(2,1)S(1)} %all_gather.3, bf16[2048,512]{1,0:T(8,128)(2,1)} %param.24), kind=kOutput, calls=%fused_computation.19 | convolution fusion | flops 25171968 | bytes 2158592 | tf_op jit(solution)/shard_map/dot_general | solution.py:53
  28.3 3.8 %multiply_add_fusion = f32[12,4,128,128]{3,2,1,0:T(8,128)S(1)} fusion(f32[12,4,128,128]{3,2,1,0:T(8,128)} %param.22, f32[12,4,128]{2,1,0:T(4,128)S(1)} %reshape.140, f32[12,4,128]{2,1,0:T(4,128)S(1)} %bitcast.85, f32[12,4,128]{2,1,0:T(4,128)S(1)} %bitcast.84), kind=kLoop, calls=%fused_computation.6 | loop fusion | flops 2359296 | bytes 6365184 | tf_op jit(solution)/shard_map/add | solution.py:62
  32.1 1.6 %copy-done.1 = f32[12,4,128,128]{3,2,1,0:T(8,128)} copy-done((f32[12,4,128,128]{3,2,1,0:T(8,128)}, f32[12,4,128,128]{3,2,1,0:T(8,128)S(1)}, u32[]{:S(2)}) %copy-start.1) | copy-done | bytes 3145752
  33.7 2.8 %fusion.51 = f32[12,4,1,128]{3,2,1,0:T(1,128)S(1)} fusion(f32[12,4,128,1]{2,3,1,0:T(1,128)S(1)} %bitcast.83, f32[12,4,128,128]{3,2,1,0:T(8,128)S(1)} %multiply_add_fusion), kind=kOutput, calls=%fused_computation.69 | convolution fusion | flops 9437184 | bytes 3194880 | tf_op jit(solution)/shard_map/bhd,bhdv->bhv/dot_general | solution.py:63
  37.1 23.9 %psum.21 = bf16[12,2048]{1,0:T(8,128)(2,1)S(1)} all-reduce(bf16[12,2048]{1,0:T(8,128)(2,1)S(1)} %convolution_convert_fusion.1), channel_id=1, replica_groups=mesh['ep'=4,'tp'=8] {'tp'}, use_global_device_ids=true, to_apply=%region_1.2 | all-reduce | flops 24576 | bytes 98304 | tf_op jit(solution)/shard_map/psum | solution.py:67
  62.0 13.9 %all_to_all.10 = bf16[4,18,2048]{2,1,0:T(8,128)(2,1)S(1)} all-to-all(bf16[4,18,2048]{2,1,0:T(8,128)(2,1)S(1)} %reshape.135), channel_id=1, replica_groups=mesh['ep'=4,'tp'=8] {'ep'}, dimensions={0} | all-to-all | bytes 589824 | tf_op jit(solution)/shard_map/all_to_all | solution.py:90
  76.0 2.9 %fusion.13 = f32[4,2,9,512]{3,2,0,1:T(8,128)S(1)} fusion(bf16[2,2048,512]{2,1,0:T(8,128)(2,1)} %param.34, bf16[4,2,9,2048]{3,0,2,1:T(4,128)(2,1)S(1)} %bitcast.78), kind=kOutput, calls=%fused_computation.13 | convolution fusion | flops 150994944 | bytes 4636672 | tf_op jit(solution)/shard_map/gecd,edf->gecf/dot_general | solution.py:98
  79.0 5.0 %fusion.9 = bf16[4,2,9,2048]{3,2,0,1:T(8,128)(2,1)S(1)} fusion(bf16[2,512,2048]{2,1,0:T(8,128)(2,1)} %param.36, bf16[2,2048,512]{2,1,0:T(8,128)(2,1)} %param.35, bf16[4,2,9,2048]{3,0,2,1:T(4,128)(2,1)S(1)} %bitcast.79, f32[4,2,9,512]{3,2,0,1:T(8,128)S(1)} %fusion.13), kind=kOutput, calls=%fused_computation.8 | convolution fusion | flops 302358528 | bytes 9125888 | tf_op jit(solution)/shard_map/gecf,efd->gecd/dot_general | solution.py:101
  84.2 0.9 copy.48
  85.2 3.5 %all-to-all-start.1 = ((bf16[4,18,2048]{2,1,0:T(8,128)(2,1)}), bf16[4,18,2048]{2,1,0:T(8,128)(2,1)S(1)}, u32[]{:S(2)}, u32[]{:S(2)}) async-start(bf16[4,18,2048]{2,1,0:T(8,128)(2,1)} %copy.48), calls=%async_computation.1 | async-start | bytes 786432 | tf_op jit(solution)/shard_map/all_to_all | solution.py:112
  88.7 1.1 fusion.53
  89.8 8.4 %all-to-all-done.1 = bf16[4,18,2048]{2,1,0:T(8,128)(2,1)S(1)} async-done(((bf16[4,18,2048]{2,1,0:T(8,128)(2,1)}), bf16[4,18,2048]{2,1,0:T(8,128)(2,1)S(1)}, u32[]{:S(2)}, u32[]{:S(2)}) %all-to-all-start.1) | async-done | bytes 294944 | tf_op jit(solution)/shard_map/all_to_all | solution.py:112
  98.5 2.0 %fusion.12 = bf16[12,2048]{1,0:T(8,128)(2,1)} fusion(f32[12,2048]{1,0:T(8,128)S(1)} %fusion.52, bf16[64,2048]{1,0:T(8,128)(2,1)S(1)} %copy-done.2, bf16[12,2048]{1,0:T(8,128)(2,1)S(1)} %add_convert_fusion, bf16[2048,64]{0,1:T(8,128)(2,1)} %param.38, f32[12,64]{1,0:T(8,128)S(1)} %fusion.53), kind=kOutput, calls=%fused_computation.11 | convolution fusion | flops 6345216 | bytes 723968 | tf_op jit(solution)/shard_map/dot_general | solution.py:111
  100.5 0.8 dynamic_slice.11
  102.0 31.7 %reduce-scatter.2.cloned.1.call-done = bf16[12,256]{1,0:T(8,128)(2,1)} async-done(((bf16[12,2048]{1,0:T(8,128)(2,1)}), bf16[12,256]{1,0:T(8,128)(2,1)}) %reduce-scatter.2.cloned.1.call-update) | async-done | bytes 6160 | tf_op jit(solution)/shard_map/reduce_scatter | solution.py:118
  133.8 0.8 fusion.41
  134.6 12.2 %all-reduce = (f32[12]{0:T(128)S(1)}, f32[12]{0:T(128)S(1)}) all-reduce(f32[12]{0:T(128)S(1)} %get-tuple-element.3, f32[12]{0:T(128)S(1)} %get-tuple-element.2), channel_id=1, replica_groups=mesh['ep'=4,'tp'=8] {'tp'}, use_global_device_ids=true, to_apply=%region_12.13 | all-reduce | flops 24 | bytes 192 | tf_op jit(solution)/shard_map/psum | solution.py:122
  146.8 1.4 add_convert_fusion.1
  (52 shorter events, 3.9 us)
Async XLA Ops:
  7.2 29.6 %copy-start = (bf16[512,2048]{1,0:T(8,128)(2,1)S(1)}, bf16[512,2048]{1,0:T(8,128)(2,1)}, u32[]{:S(2)}) copy-start(bf16[512,2048]{1,0:T(8,128)(2,1)} %param.29) | copy-start | bytes 6291460
  22.1 6.1 %copy-start.3 = (f32[4,128]{1,0:T(4,128)S(1)}, f32[4,128]{1,0:T(4,128)}, u32[]{:S(2)}) copy-start(f32[4,128]{1,0:T(4,128)} %param.23) | copy-start | bytes 6148
  32.1 1.7 %copy-start.1 = (f32[12,4,128,128]{3,2,1,0:T(8,128)}, f32[12,4,128,128]{3,2,1,0:T(8,128)S(1)}, u32[]{:S(2)}) copy-start(f32[12,4,128,128]{3,2,1,0:T(8,128)S(1)} %multiply_add_fusion) | copy-start | bytes 9437188
  32.1 4.5 %copy-start.6 = (f32[128]{0:T(128)S(1)}, f32[128]{0:T(128)}, u32[]{:S(2)}) copy-start(f32[128]{0:T(128)} %param.28) | copy-start | bytes 1540
  32.1 29.4 %copy-start.4 = (f32[2048]{0:T(1024)S(1)}, f32[2048]{0:T(1024)}, u32[]{:S(2)}) copy-start(f32[2048]{0:T(1024)} %param.31) | copy-start | bytes 24580
  32.1 29.4 %copy-start.5 = (f32[2048]{0:T(1024)S(1)}, f32[2048]{0:T(1024)}, u32[]{:S(2)}) copy-start(f32[2048]{0:T(1024)} %param.30) | copy-start | bytes 24580
  84.0 14.5 %copy-start.2 = (bf16[64,2048]{1,0:T(8,128)(2,1)S(1)}, bf16[64,2048]{1,0:T(8,128)(2,1)}, u32[]{:S(2)}) copy-start(bf16[64,2048]{1,0:T(8,128)(2,1)} %param.39) | copy-start | bytes 786436
  85.2 13.0 %all-to-all-start.1 = ((bf16[4,18,2048]{2,1,0:T(8,128)(2,1)}), bf16[4,18,2048]{2,1,0:T(8,128)(2,1)S(1)}, u32[]{:S(2)}, u32[]{:S(2)}) async-start(bf16[4,18,2048]{2,1,0:T(8,128)(2,1)} %copy.48), calls=%async_computation.1 | async-start | bytes 786432 | tf_op jit(solution)/shard_map/all_to_all | solution.py:112
  88.6 45.2 %reduce-scatter.2.cloned.1.call-start = ((), (), s32[]{:S(2)}) async-start(), calls=%async_computation.3 | async-start | bytes 73728 | tf_op jit(solution)/shard_map/reduce_scatter | solution.py:118
Sparse Core Ops, SparseCore 0:
  100.6 33.1 reduce-scatter.1
where the time goes:
time: 156 us; the launch traced here: 155 us
  blocking collectives  60.6 us (39%)
  waiting for transfers between devices  40.1 us (26%)
  matrix products  22.5 us (14%)
  between operations  14.3 us (9%)
  other arithmetic  7.16 us (5%)
  local copies, waits for them, and re-layouts  6.75 us (4%)
  starting transfers between devices  3.5 us (2%)
    reduce_scatter x1, waiting for transfers between devices, local(): lax.psum_scatter((routed_partial + shared_part).astype(jnp.bfloat16), 'tp...  31.7 us
    psum x1, blocking collectives, local(): summed = lax.psum(branch.astype(jnp.bfloat16), 'tp').astype(jnp.float32)  23.9 us
    all_to_all x1, blocking collectives, local(): lax.all_to_all(picked.astype(jnp.bfloat16).reshape(n_ep, local_experts *...  13.9 us
    psum x1, blocking collectives, local(): lax.psum((jnp.sum(final_in, -1), jnp.sum(final_in * final_in, -1)), 'tp')  12.2 us
    all_gather x1, blocking collectives, local(): rows_full = lax.all_gather(hidden_in, 'tp', axis=1, tiled=True)  10.7 us
    all_to_all x1, waiting for transfers between devices, local(): lax.all_to_all(expert_part, 'ep', split_axis=0, concat_axis=0, tiled=True)  8.36 us
    dot_general x4, matrix products, project(): product = jnp.dot(rows_full, weight, preferred_element_type=jnp.float32)  7.85 us
    dot_general x1, matrix products, local(): jnp.einsum('gecf,efd->gecd', hidden_part, exp_down, preferred_element_typ...  4.99 us
  transfers between devices with their start and end apart: 2, of which 2 were waited for; matrix products, arithmetic and copies ran while one was open for 2% of the time, Pallas kernels for 0%

commit v1 on v0

--- a/solution.py
+++ b/solution.py
@@ -64,7 +64,7 @@
     normed = readout * lax.rsqrt(jnp.mean(readout * readout, -1, keepdims=True) + EPS) * head_gain
     mixed = (normed * out_gate).astype(jnp.bfloat16).reshape(seq_count, heads_dev * head_size)
     branch = jnp.dot(mixed, w_out, preferred_element_type=jnp.float32)
-    summed = lax.psum(branch.astype(jnp.bfloat16), "tp").astype(jnp.float32)
+    summed = jnp.sum(lax.all_gather(branch.astype(jnp.bfloat16), "tp"), axis=0).astype(jnp.float32)
     residual = ALPHA * rows_full.astype(jnp.float32) + summed
     average = jnp.mean(residual, -1, keepdims=True)
     centered = residual - average

time: 156 us -> 143 us (0.917)
  blocking collectives: 60.6 us -> 49.4 us
  waiting for transfers between devices: 40.1 us -> 38.3 us
    psum x1 -> x0, blocking collectives: 23.9 us -> none  [local(): summed = lax.psum(branch.astype(jnp.bfloat16), 'tp').astype(jnp.float32)]
    all_gather x0 -> x1, blocking collectives: none -> 9.67 us  [local(): lax.all_gather(branch.astype(jnp.bfloat16), 'tp')]
    reduce_scatter x1, waiting for transfers between devices: 31.7 us -> 28.1 us  [local(): lax.psum_scatter((routed_partial + shared_part).astype(jnp.bfloat16), 'tp...]
    all_to_all x1, blocking collectives: 13.9 us -> 16.9 us  [local(): lax.all_to_all(picked.astype(jnp.bfloat16).reshape(n_ep, local_experts *...]
    all_to_all x1, waiting for transfers between devices: 8.36 us -> 10.1 us  [local(): lax.all_to_all(expert_part, 'ep', split_axis=0, concat_axis=0, tiled=True)]
where the time goes in v1:
time: 143 us; the launch traced here: 142 us
  blocking collectives  49.4 us (35%)
  waiting for transfers between devices  38.3 us (27%)
  matrix products  22.5 us (16%)
  between operations  14.3 us (10%)
  other arithmetic  7.25 us (5%)
  local copies, waits for them, and re-layouts  6.77 us (5%)
  starting transfers between devices  3.5 us (2%)
    reduce_scatter x1, waiting for transfers between devices, local(): lax.psum_scatter((routed_partial + shared_part).astype(jnp.bfloat16), 'tp...  28.1 us
    all_to_all x1, blocking collectives, local(): lax.all_to_all(picked.astype(jnp.bfloat16).reshape(n_ep, local_experts *...  16.9 us
    psum x1, blocking collectives, local(): lax.psum((jnp.sum(final_in, -1), jnp.sum(final_in * final_in, -1)), 'tp')  12.1 us
    all_gather x1, blocking collectives, local(): rows_full = lax.all_gather(hidden_in, 'tp', axis=1, tiled=True)  10.7 us
    all_to_all x1, waiting for transfers between devices, local(): lax.all_to_all(expert_part, 'ep', split_axis=0, concat_axis=0, tiled=True)  10.1 us
    all_gather x1, blocking collectives, local(): lax.all_gather(branch.astype(jnp.bfloat16), 'tp')  9.67 us
    dot_general x4, matrix products, project(): product = jnp.dot(rows_full, weight, preferred_element_type=jnp.float32)  7.85 us
    dot_general x1, matrix products, local(): jnp.einsum('gecf,efd->gecd', hidden_part, exp_down, preferred_element_typ...  5 us
  transfers between devices with their start and end apart: 2, of which 2 were waited for; matrix products, arithmetic and copies ran while one was open for 2% of the time, Pallas kernels for 0%

profile of v1, /device:TPU:0, one launch (start us, length us, event | category | flops | bytes accessed | tf_op | source)
XLA Modules:
  0.0 142.0 jit_solution(15201163073139681216)
XLA Ops:
  7.2 0.9 copy.41
  8.6 0.8 copy.43
  9.4 10.7 %all_gather.9 = bf16[12,2048]{1,0:T(8,128)(2,1)S(1)} all-gather(bf16[12,256]{1,0:T(8,128)(2,1)} %param.21), channel_id=1, replica_groups=mesh['ep'=4,'tp'=8] {'tp'}, dimensions={1}, use_global_device_ids=true | all-gather | bytes 55296 | tf_op jit(solution)/shard_map/all_gather | solution.py:50
  20.1 2.0 %convolution_convert_fusion.2 = bf16[12,512]{1,0:T(8,128)(2,1)S(1)} fusion(bf16[12,2048]{1,0:T(8,128)(2,1)S(1)} %all_gather.9, bf16[2048,512]{1,0:T(8,128)(2,1)} %param.27), kind=kOutput, calls=%fused_computation.18 | convolution fusion | flops 25171968 | bytes 2158592 | tf_op jit(solution)/shard_map/dot_general | solution.py:53
  22.1 2.0 %convolution_convert_fusion.5 = bf16[12,512]{1,0:T(8,128)(2,1)S(1)} fusion(bf16[12,2048]{1,0:T(8,128)(2,1)S(1)} %all_gather.9, bf16[2048,512]{1,0:T(8,128)(2,1)} %param.26), kind=kOutput, calls=%fused_computation.21 | convolution fusion | flops 25171968 | bytes 2158592 | tf_op jit(solution)/shard_map/dot_general | solution.py:53
  24.1 2.0 %convolution_convert_fusion.3 = bf16[12,512]{1,0:T(8,128)(2,1)S(1)} fusion(bf16[12,2048]{1,0:T(8,128)(2,1)S(1)} %all_gather.9, bf16[2048,512]{1,0:T(8,128)(2,1)} %param.25), kind=kOutput, calls=%fused_computation.19 | convolution fusion | flops 25171968 | bytes 2158592 | tf_op jit(solution)/shard_map/dot_general | solution.py:53
  26.1 2.0 %convolution_convert_fusion.4 = bf16[12,512]{1,0:T(8,128)(2,1)S(1)} fusion(bf16[12,2048]{1,0:T(8,128)(2,1)S(1)} %all_gather.9, bf16[2048,512]{1,0:T(8,128)(2,1)} %param.24), kind=kOutput, calls=%fused_computation.20 | convolution fusion | flops 25171968 | bytes 2158592 | tf_op jit(solution)/shard_map/dot_general | solution.py:53
  28.3 3.8 %multiply_add_fusion = f32[12,4,128,128]{3,2,1,0:T(8,128)S(1)} fusion(f32[12,4,128,128]{3,2,1,0:T(8,128)} %param.22, f32[12,4,128]{2,1,0:T(4,128)S(1)} %reshape.140, f32[12,4,128]{2,1,0:T(4,128)S(1)} %bitcast.87, f32[12,4,128]{2,1,0:T(4,128)S(1)} %bitcast.86), kind=kLoop, calls=%fused_computation.6 | loop fusion | flops 2359296 | bytes 6365184 | tf_op jit(solution)/shard_map/add | solution.py:62
  32.1 1.6 %copy-done.1 = f32[12,4,128,128]{3,2,1,0:T(8,128)} copy-done((f32[12,4,128,128]{3,2,1,0:T(8,128)}, f32[12,4,128,128]{3,2,1,0:T(8,128)S(1)}, u32[]{:S(2)}) %copy-start.1) | copy-done | bytes 3145752
  33.7 2.8 %fusion.52 = f32[12,4,1,128]{3,2,1,0:T(1,128)S(1)} fusion(f32[12,4,128,1]{2,3,1,0:T(1,128)S(1)} %bitcast.85, f32[12,4,128,128]{3,2,1,0:T(8,128)S(1)} %multiply_add_fusion), kind=kOutput, calls=%fused_computation.70 | convolution fusion | flops 9437184 | bytes 3194880 | tf_op jit(solution)/shard_map/bhd,bhdv->bhv/dot_general | solution.py:63
  37.1 9.7 %all-gather.1 = bf16[8,12,2048]{2,1,0:T(8,128)(2,1)S(1)} all-gather(bf16[1,12,2048]{2,1,0:T(8,128)(2,1)S(1)} %fusion.13), channel_id=2, replica_groups=mesh['ep'=4,'tp'=8] {'tp'}, dimensions={0}, use_global_device_ids=true | all-gather | bytes 442368 | tf_op jit(solution)/shard_map/all_gather | solution.py:67
  47.9 16.9 %all_to_all.10 = bf16[4,18,2048]{2,1,0:T(8,128)(2,1)S(1)} all-to-all(bf16[4,18,2048]{2,1,0:T(8,128)(2,1)S(1)} %reshape.135), channel_id=1, replica_groups=mesh['ep'=4,'tp'=8] {'ep'}, dimensions={0} | all-to-all | bytes 589824 | tf_op jit(solution)/shard_map/all_to_all | solution.py:90
  65.0 2.9 %fusion.14 = f32[4,2,9,512]{3,2,0,1:T(8,128)S(1)} fusion(bf16[2,2048,512]{2,1,0:T(8,128)(2,1)} %param.34, bf16[4,2,9,2048]{3,0,2,1:T(4,128)(2,1)S(1)} %bitcast.80), kind=kOutput, calls=%fused_computation.14 | convolution fusion | flops 150994944 | bytes 4636672 | tf_op jit(solution)/shard_map/gecd,edf->gecf/dot_general | solution.py:98
  67.9 5.0 %fusion.9 = bf16[4,2,9,2048]{3,2,0,1:T(8,128)(2,1)S(1)} fusion(bf16[2,512,2048]{2,1,0:T(8,128)(2,1)} %param.36, bf16[2,2048,512]{2,1,0:T(8,128)(2,1)} %param.35, bf16[4,2,9,2048]{3,0,2,1:T(4,128)(2,1)S(1)} %bitcast.81, f32[4,2,9,512]{3,2,0,1:T(8,128)S(1)} %fusion.14), kind=kOutput, calls=%fused_computation.8 | convolution fusion | flops 302358528 | bytes 9125888 | tf_op jit(solution)/shard_map/gecf,efd->gecd/dot_general | solution.py:101
  73.2 0.9 copy.48
  74.1 3.5 %all-to-all-start.1 = ((bf16[4,18,2048]{2,1,0:T(8,128)(2,1)}), bf16[4,18,2048]{2,1,0:T(8,128)(2,1)S(1)}, u32[]{:S(2)}, u32[]{:S(2)}) async-start(bf16[4,18,2048]{2,1,0:T(8,128)(2,1)} %copy.48), calls=%async_computation.1 | async-start | bytes 786432 | tf_op jit(solution)/shard_map/all_to_all | solution.py:112
  77.6 1.1 fusion.54
  78.7 10.1 %all-to-all-done.1 = bf16[4,18,2048]{2,1,0:T(8,128)(2,1)S(1)} async-done(((bf16[4,18,2048]{2,1,0:T(8,128)(2,1)}), bf16[4,18,2048]{2,1,0:T(8,128)(2,1)S(1)}, u32[]{:S(2)}, u32[]{:S(2)}) %all-to-all-start.1) | async-done | bytes 294944 | tf_op jit(solution)/shard_map/all_to_all | solution.py:112
  89.2 2.0 %fusion.12 = bf16[12,2048]{1,0:T(8,128)(2,1)} fusion(f32[12,2048]{1,0:T(8,128)S(1)} %fusion.53, bf16[64,2048]{1,0:T(8,128)(2,1)S(1)} %copy-done.2, bf16[12,2048]{1,0:T(8,128)(2,1)S(1)} %add_convert_fusion, bf16[2048,64]{0,1:T(8,128)(2,1)} %param.38, f32[12,64]{1,0:T(8,128)S(1)} %fusion.54), kind=kOutput, calls=%fused_computation.11 | convolution fusion | flops 6345216 | bytes 723968 | tf_op jit(solution)/shard_map/dot_general | solution.py:111
  91.2 0.8 dynamic_slice.11
  92.7 28.1 %reduce-scatter.2.cloned.1.call-done = bf16[12,256]{1,0:T(8,128)(2,1)} async-done(((bf16[12,2048]{1,0:T(8,128)(2,1)}), bf16[12,256]{1,0:T(8,128)(2,1)}) %reduce-scatter.2.cloned.1.call-update) | async-done | bytes 6160 | tf_op jit(solution)/shard_map/reduce_scatter | solution.py:118
  120.9 0.8 fusion.42
  121.7 12.1 %all-reduce = (f32[12]{0:T(128)S(1)}, f32[12]{0:T(128)S(1)}) all-reduce(f32[12]{0:T(128)S(1)} %get-tuple-element.3, f32[12]{0:T(128)S(1)} %get-tuple-element.2), channel_id=1, replica_groups=mesh['ep'=4,'tp'=8] {'tp'}, use_global_device_ids=true, to_apply=%region_12.13 | all-reduce | flops 24 | bytes 192 | tf_op jit(solution)/shard_map/psum | solution.py:122
  133.8 1.4 add_convert_fusion.1
  (53 shorter events, 4.0 us)
Async XLA Ops:
  7.2 29.6 %copy-start = (bf16[512,2048]{1,0:T(8,128)(2,1)S(1)}, bf16[512,2048]{1,0:T(8,128)(2,1)}, u32[]{:S(2)}) copy-start(bf16[512,2048]{1,0:T(8,128)(2,1)} %param.29) | copy-start | bytes 6291460
  22.1 6.1 %copy-start.3 = (f32[4,128]{1,0:T(4,128)S(1)}, f32[4,128]{1,0:T(4,128)}, u32[]{:S(2)}) copy-start(f32[4,128]{1,0:T(4,128)} %param.23) | copy-start | bytes 6148
  32.1 1.7 %copy-start.1 = (f32[12,4,128,128]{3,2,1,0:T(8,128)}, f32[12,4,128,128]{3,2,1,0:T(8,128)S(1)}, u32[]{:S(2)}) copy-start(f32[12,4,128,128]{3,2,1,0:T(8,128)S(1)} %multiply_add_fusion) | copy-start | bytes 9437188
  32.1 4.5 %copy-start.6 = (f32[128]{0:T(128)S(1)}, f32[128]{0:T(128)}, u32[]{:S(2)}) copy-start(f32[128]{0:T(128)} %param.28) | copy-start | bytes 1540
  33.7 13.6 %copy-start.4 = (f32[2048]{0:T(1024)S(1)}, f32[2048]{0:T(1024)}, u32[]{:S(2)}) copy-start(f32[2048]{0:T(1024)} %param.31) | copy-start | bytes 24580
  33.7 13.7 %copy-start.5 = (f32[2048]{0:T(1024)S(1)}, f32[2048]{0:T(1024)}, u32[]{:S(2)}) copy-start(f32[2048]{0:T(1024)} %param.30) | copy-start | bytes 24580
  72.9 16.3 %copy-start.2 = (bf16[64,2048]{1,0:T(8,128)(2,1)S(1)}, bf16[64,2048]{1,0:T(8,128)(2,1)}, u32[]{:S(2)}) copy-start(bf16[64,2048]{1,0:T(8,128)(2,1)} %param.39) | copy-start | bytes 786436
  74.1 14.8 %all-to-all-start.1 = ((bf16[4,18,2048]{2,1,0:T(8,128)(2,1)}), bf16[4,18,2048]{2,1,0:T(8,128)(2,1)S(1)}, u32[]{:S(2)}, u32[]{:S(2)}) async-start(bf16[4,18,2048]{2,1,0:T(8,128)(2,1)} %copy.48), calls=%async_computation.1 | async-start | bytes 786432 | tf_op jit(solution)/shard_map/all_to_all | solution.py:112
  77.5 43.3 %reduce-scatter.2.cloned.1.call-start = ((), (), s32[]{:S(2)}) async-start(), calls=%async_computation.3 | async-start | bytes 73728 | tf_op jit(solution)/shard_map/reduce_scatter | solution.py:118
Sparse Core Ops, SparseCore 0:
  91.3 29.4 reduce-scatter.1
